TPU v7x, 32 devices: a whole 2x2x4 slice. The times are simulated.
32 devices in a mesh: grp: 2 (over y), sp: 8 (over z, core), tp: 2 (over x).
Axes of the slice: x: 2, y: 2, z: 4, core: 2. Of those that a mesh axis runs over, the one named last changes fastest.
Arguments:
- query_plain: bfloat16 [2560, 1024], P(('grp', 'sp'), 'tp'), parts along dimension 0, may hold values from -6 to 6
- query_turn: bfloat16 [2560, 512], P(('grp', 'sp'), 'tp'), parts along dimension 0, may hold values from -40 to 40, as said below
- latent: bfloat16 [2560, 512], P(('grp', 'sp')), parts along dimension 0, may hold values from -6 to 6
- key_turn: bfloat16 [2560, 64], P(('grp', 'sp')), parts along dimension 0, may hold values from -40 to 40, as said below
- latent_norm_scale: bfloat16 [512], replicated, may hold values from 0.099609375 to 1.8984375
- plain_key_matrix: bfloat16 [512, 1024], P(None, 'tp'), may hold values from -0.25 to 0.25
- value_matrix: bfloat16 [512, 1024], P(None, 'tp'), may hold values from -0.25 to 0.25
- residual: bfloat16 [2560, 2048], P(('grp', 'sp', 'tp')), parts along dimension 0, may hold values from -6 to 6
- out_weight: bfloat16 [1024, 2048], replicated, may hold values from -6 to 6
- ffn_gain: bfloat16 [2048], replicated, may hold values from 0.099609375 to 1.8984375
- gate_weight: bfloat16 [8, 2048, 1024], P('sp', None, 'tp'), may hold values from -1 to 1
- up_weight: bfloat16 [8, 2048, 1024], P('sp', None, 'tp'), may hold values from -1 to 1
- down_weight: bfloat16 [8, 1024, 2048], P('sp', 'tp'), may hold values from -0.0625 to 0.0625
- routes: int32 [2560, 4], P(('grp', 'sp', 'tp')), parts along dimension 0, may hold values from 0 to 7, all different within a row; in each aligned block of 80 rows (0 to 79, 80 to 159, ...) at most 60 rows name the same one
- route_weights: float32 [2560, 4], P(('grp', 'sp', 'tp')), parts along dimension 0, may hold values from 0.1 to 0.6
Outputs:
- mixed: bfloat16 [2560, 2048], P(('grp', 'sp', 'tp')), parts along dimension 0
There are 2 independent parts, one for each index of `grp`. A program takes and returns all parts, laid end to end along the dimension named above; an argument that names none is the same for every part. Nothing has to cross between parts.
Inputs may be any that keep to these rules, and one draw needn't show every extreme that they name: `query_turn`: in the hidden draw some rows are large. `key_turn`: in the hidden draw some rows are large. `routes`: each row names 4 different experts. In each aligned block of 80 rows (the rows of one device) no expert is named more than 60 times, a bound that some block reaches.
All inputs are finite; a program needn't handle non-finite values.
Results may differ from a plain program's by a relative error of at most 0.015.
Values may be sent and summed in bfloat16 or wider, within the bound.
A program may use at most 128 MiB of HBM per device.

v0:
```python
import jax
import jax.numpy as jnp
from jax import lax
from jax.sharding import PartitionSpec as P

PLAIN_HEAD_WIDTH = 128
QK_ROPE = 64
VALUE_WIDTH = 128
GRID_W = 64
theta = 10000.0
eps = 1e-06
limit = 7.0
slope = 1.702


def turn(vector, row_shift, col_shift):
    width = vector.shape[-1]
    count = width // 4
    half = width // 2
    freqs = theta ** (-jnp.arange(count, dtype=jnp.float32) / count)
    extra = (1,) * (vector.ndim - 2)
    pieces = []
    for portion, shift in ((vector[..., :half], row_shift), (vector[..., half:], col_shift)):
        angle = (shift.astype(jnp.float32)[:, None] * freqs[None, :]).reshape(
            (shift.shape[0],) + extra + (count,)
        )
        lower = portion[..., :count]
        upper = portion[..., count:]
        pieces.append(
            jnp.concatenate(
                [
                    lower * jnp.cos(angle) - upper * jnp.sin(angle),
                    lower * jnp.sin(angle) + upper * jnp.cos(angle),
                ],
                axis=-1,
            )
        )
    return jnp.concatenate(pieces, axis=-1)


def norm_scale(values, gain):
    wide = values.astype(jnp.float32)
    return (
        wide
        * lax.rsqrt(jnp.mean(wide * wide, axis=-1, keepdims=True) + eps)
        * gain.astype(jnp.float32)
    )


def expert_active(rows, gate_w, up_w):
    gate_pre = jnp.minimum(jnp.dot(rows, gate_w, preferred_element_type=jnp.float32), limit)
    up_pre = jnp.clip(jnp.dot(rows, up_w, preferred_element_type=jnp.float32), -limit, limit)
    return ((up_pre + 1.0) * gate_pre * jax.nn.sigmoid(slope * gate_pre)).astype(jnp.bfloat16)


def on_device(
    query_plain,
    query_turn,
    latent,
    key_turn,
    latent_norm_scale,
    plain_key_matrix,
    value_matrix,
    residual,
    out_weight,
    ffn_gain,
    gate_weight,
    up_weight,
    down_weight,
    routes,
    route_weights,
):
    tok_dev = latent.shape[0]
    heads_dev = query_plain.shape[1] // PLAIN_HEAD_WIDTH
    model_width = residual.shape[1]
    place = lax.axis_index("sp") * tok_dev + jnp.arange(tok_dev, dtype=jnp.int32)
    grid_row = place // GRID_W
    grid_col = place % GRID_W
    normed_latent = norm_scale(latent, latent_norm_scale).astype(jnp.bfloat16)
    key_rot = turn(key_turn.astype(jnp.float32), grid_row, grid_col).astype(jnp.bfloat16)
    expert_ids = jnp.arange(lax.axis_size("sp"), dtype=jnp.int32)
    share = jnp.sum(
        route_weights[..., None] * (routes[..., None] == expert_ids).astype(jnp.float32), axis=1
    )
    latent_width = latent.shape[1]
    sent = jnp.concatenate([normed_latent, key_rot], axis=1)
    everyone = lax.all_gather(sent, "sp", axis=0, tiled=True)
    shares = lax.all_gather(share, ("sp", "tp"), axis=0, tiled=True)
    all_latent = everyone[:, :latent_width]
    all_rot = everyone[:, latent_width:]
    keys = jnp.dot(all_latent, plain_key_matrix, preferred_element_type=jnp.float32).astype(
        jnp.bfloat16
    )
    values = jnp.dot(all_latent, value_matrix, preferred_element_type=jnp.float32).astype(
        jnp.bfloat16
    )
    query_rot = turn(
        query_turn.astype(jnp.float32).reshape(tok_dev, heads_dev, QK_ROPE), grid_row, grid_col
    ).astype(jnp.bfloat16)
    scale = (PLAIN_HEAD_WIDTH + QK_ROPE) ** (-0.5)
    attended = []
    for head in range(heads_dev):
        span = slice(head * PLAIN_HEAD_WIDTH, (head + 1) * PLAIN_HEAD_WIDTH)
        scores = (
            jnp.einsum(
                "qd,kd->qk", query_plain[:, span], keys[:, span], preferred_element_type=jnp.float32
            )
            + jnp.einsum(
                "qd,kd->qk", query_rot[:, head], all_rot, preferred_element_type=jnp.float32
            )
        ) * scale
        weights = jnp.exp(scores - jnp.max(scores, axis=1, keepdims=True))
        summed = jnp.dot(
            weights.astype(jnp.bfloat16),
            values[:, head * VALUE_WIDTH : (head + 1) * VALUE_WIDTH],
            preferred_element_type=jnp.float32,
        )
        attended.append((summed / jnp.sum(weights, axis=1, keepdims=True)).astype(jnp.bfloat16))
    attended = jnp.concatenate(attended, axis=1)
    rows_dev = residual.shape[0]
    group = lax.axis_size("tp")
    swapped = lax.all_to_all(
        attended.reshape(group, rows_dev, heads_dev * VALUE_WIDTH),
        "tp",
        split_axis=0,
        concat_axis=0,
        tiled=True,
    )
    own_rows = jnp.transpose(swapped, (1, 0, 2)).reshape(rows_dev, group * heads_dev * VALUE_WIDTH)
    projected = jnp.dot(own_rows, out_weight, preferred_element_type=jnp.float32)
    hidden = (residual.astype(jnp.float32) + projected).astype(jnp.bfloat16)
    normed = norm_scale(hidden, ffn_gain).astype(jnp.bfloat16)
    rows = lax.all_gather(normed, ("sp", "tp"), axis=0, tiled=True)
    active = expert_active(rows, gate_weight[0], up_weight[0])
    product = jnp.dot(active, down_weight[0], preferred_element_type=jnp.float32)
    own_share = jnp.sum(
        jnp.where(expert_ids[None, :] == lax.axis_index("sp"), shares, 0.0), axis=1, keepdims=True
    )
    mixture = lax.psum_scatter(
        (own_share * product).astype(jnp.bfloat16), ("sp", "tp"), scatter_dimension=0, tiled=True
    )
    return (hidden.astype(jnp.float32) + mixture.astype(jnp.float32)).astype(jnp.bfloat16)


def solution(mesh):
    placed = (
        P(("grp", "sp"), "tp"),
        P(("grp", "sp"), "tp"),
        P(("grp", "sp"), None),
        P(("grp", "sp"), None),
        P(),
        P(None, "tp"),
        P(None, "tp"),
        P(("grp", "sp", "tp"), None),
        P(),
        P(),
        P("sp", None, "tp"),
        P("sp", None, "tp"),
        P("sp", "tp", None),
        P(("grp", "sp", "tp"), None),
        P(("grp", "sp", "tp"), None),
    )
    return jax.shard_map(
        on_device,
        mesh=mesh,
        in_specs=placed,
        out_specs=P(("grp", "sp", "tp"), None),
        check_vma=False,
    )
```

profile of v0, /device:TPU:0, one launch (start us, length us, event | category | flops | bytes accessed | tf_op | source)
XLA Modules:
  0.0 219.9 jit_solution(17451108675109857187)
XLA Ops:
  6.6 1.2 fusion.37
  7.8 0.7 convert_element_type.92
  8.5 0.8 convert_element_type.94
  9.2 0.2 multiply_cosine_fusion
  9.5 0.1 copy.52
  9.6 0.1 copy.51
  9.7 0.1 copy.53
  9.8 0.1 copy.54
  9.9 1.0 fusion.39
  11.0 0.8 concatenate.13
  11.8 0.0 all-gather.4.cloned.1.call-update
  11.8 1.0 copy.55
  12.9 27.4 %all-gather.4.cloned.1.call-done = bf16[1280,576]{1,0:T(8,128)(2,1)} async-done(((bf16[160,576]{1,0:T(8,128)(2,1)}), bf16[1280,576]{1,0:T(8,128)(2,1)}) %all-gather.4.cloned.1.call-update) | async-done | bytes 1474576 | tf_op jit(solution)/shard_map/all_gather | solution.py:87
  40.3 2.2 convolution_convert_fusion.1
  42.5 0.3 convolution_bitcast_fusion
  42.8 0.3 convolution_bitcast_fusion.1
  43.1 0.3 convolution_bitcast_fusion.2
  43.3 0.3 convolution_bitcast_fusion.3
  43.6 0.3 copy-done.1
  43.9 0.4 fusion.63
  44.3 0.3 fusion.27
  44.6 0.8 convolution_convert_fusion
  45.5 0.3 fusion.18
  45.8 0.4 fusion.64
  46.2 0.3 fusion.25
  46.5 0.3 fusion.17
  46.8 0.4 fusion.66
  47.2 0.3 fusion.21
  47.5 0.3 fusion.15
  47.9 0.4 fusion.65
  48.3 0.3 fusion.23
  48.6 0.3 fusion.16
  48.9 0.7 pad_maximum_fusion
  49.6 3.4 %all-to-all-start = ((bf16[2,80,512]{2,1,0:T(8,128)(2,1)}), bf16[2,80,512]{2,1,0:T(8,128)(2,1)S(1)}, u32[]{:S(2)}, u32[]{:S(2)}) async-start(bf16[2,80,512]{2,1,0:T(8,128)(2,1)} %bitcast.10), calls=%async_computation | async-start | bytes 327680 | tf_op jit(solution)/shard_map/all_to_all | solution.py:122
  53.0 0.0 all-gather.6.cloned.1.call-start
  53.1 4.7 %all-to-all-done = bf16[2,80,512]{2,1,0:T(8,128)(2,1)S(1)} async-done(((bf16[2,80,512]{2,1,0:T(8,128)(2,1)}), bf16[2,80,512]{2,1,0:T(8,128)(2,1)S(1)}, u32[]{:S(2)}, u32[]{:S(2)}) %all-to-all-start) | async-done | bytes 163872 | tf_op jit(solution)/shard_map/all_to_all | solution.py:122
  57.8 3.2 %multiply_reduce_fusion = (f32[80]{0:T(128)S(1)}, f32[80,2048]{1,0:T(8,128)S(1)}) fusion(bf16[80,1024]{1,0:T(8,128)(2,1)S(1)} %bitcast.54, bf16[1024,2048]{1,0:T(8,128)(2,1)} %param.23, bf16[80,2048]{1,0:T(8,128)(2,1)S(1)} %copy-done.2), kind=kOutput, calls=%fused_computation.51 | convolution fusion | flops 336527296 | bytes 5341504 | tf_op jit(solution)/shard_map/dot_general | solution.py:130
  61.0 0.9 multiply_convert_fusion.1
  61.9 0.0 all-gather.6.cloned.1.call-update
  61.9 0.0 reduce-scatter.2.cloned.1.call-start
  62.0 29.8 %all-gather = f32[16,80,8]{1,2,0:T(8,128)S(1)} all-gather(f32[1,80,8]{1,2,0:T(8,128)S(1)} %bitcast.57), channel_id=1, replica_groups=mesh['grp'=2,'sp'=8,'tp'=2] {'sp','tp'}, dimensions={0}, use_global_device_ids=true | all-gather | bytes 43520 | tf_op jit(solution)/shard_map/all_gather | solution.py:88
  91.8 0.1 reshape.193
  91.9 0.1 select_reduce_fusion
  92.0 24.3 %all-gather.6.cloned.1.call-done = bf16[1280,2048]{1,0:T(8,128)(2,1)} async-done(((bf16[80,2048]{1,0:T(8,128)(2,1)}), bf16[1280,2048]{1,0:T(8,128)(2,1)}) %all-gather.6.cloned.1.call-update) | async-done | bytes 5242896 | tf_op jit(solution)/shard_map/all_gather | solution.py:133
  116.4 7.6 %convolution_minimum_fusion = f32[1280,512]{1,0:T(8,128)} fusion(bf16[1280,2048]{1,0:T(8,128)(2,1)} %all-gather.6.cloned.1.call-done, bf16[1,2048,512]{2,1,0:T(8,128)(2,1)} %param.25), kind=kOutput, calls=%fused_computation.2 | convolution fusion | flops 2685009920 | bytes 9961472 | tf_op jit(solution)/shard_map/dot_general | solution.py:51
  123.9 10.5 %multiply_convert_fusion = bf16[1280,2048]{1,0:T(8,128)(2,1)} fusion(f32[1280]{0:T(1024)S(1)} %select_reduce_fusion, bf16[1,512,2048]{2,1,0:T(8,128)(2,1)S(1)} %copy-done, f32[1280,512]{1,0:T(8,128)} %convolution_minimum_fusion, bf16[1280,2048]{1,0:T(8,128)(2,1)} %all-gather.6.cloned.1.call-done, bf16[1,2048,512]{2,1,0:T(8,128)(2,1)} %param.26), kind=kOutput, calls=%fused_computation | convolution fusion | flops 5379850240 | bytes 17306624 | tf_op jit(solution)/shard_map/dot_general | solution.py:135
  134.4 77.2 %reduce-scatter.2.cloned.1.call-done = bf16[80,2048]{1,0:T(8,128)(2,1)} async-done(((bf16[1280,2048]{1,0:T(8,128)(2,1)}), bf16[80,2048]{1,0:T(8,128)(2,1)}) %reduce-scatter.2.cloned.1.call-update) | async-done | bytes 327696 | tf_op jit(solution)/shard_map/reduce_scatter | solution.py:139
  211.6 1.8 add_convert_fusion
  (31 shorter events, 0.2 us)
Async XLA Ops:
  6.5 117.4 %copy-start = (bf16[1,512,2048]{2,1,0:T(8,128)(2,1)S(1)}, bf16[1,512,2048]{2,1,0:T(8,128)(2,1)}, u32[]{:S(2)}) copy-start(bf16[1,512,2048]{2,1,0:T(8,128)(2,1)} %param.27) | copy-start | bytes 6291460
  6.5 33.8 %copy-start.7 = (bf16[512,512]{1,0:T(8,128)(2,1)S(1)}, bf16[512,512]{1,0:T(8,128)(2,1)}, u32[]{:S(2)}) copy-start(bf16[512,512]{1,0:T(8,128)(2,1)} %param.20) | copy-start | bytes 1572868
  6.5 33.8 %all-gather.4.cloned.1.call-start = ((), (), s32[]{:S(2)}) async-start(), calls=%async_computation.2 | async-start | bytes 1843200 | tf_op jit(solution)/shard_map/all_gather | solution.py:87
  12.9 29.6 %copy-start.3 = (bf16[160,512]{1,0:T(8,128)(2,1)S(1)}, bf16[160,512]{1,0:T(8,128)(2,1)}, u32[]{:S(2)}) copy-start(bf16[160,512]{1,0:T(8,128)(2,1)} %param.15) | copy-start | bytes 491524
  42.5 1.4 copy-start.1
  43.3 1.3 copy-start.8
  47.9 5.2 %copy-start.4 = (bf16[2048]{0:T(1024)(128)(2,1)S(1)}, bf16[2048]{0:T(1024)(128)(2,1)}, u32[]{:S(2)}) copy-start(bf16[2048]{0:T(1024)(128)(2,1)} %param.24) | copy-start | bytes 12292
  47.9 9.9 %copy-start.2 = (bf16[80,2048]{1,0:T(8,128)(2,1)S(1)}, bf16[80,2048]{1,0:T(8,128)(2,1)}, u32[]{:S(2)}) copy-start(bf16[80,2048]{1,0:T(8,128)(2,1)} %param.22) | copy-start | bytes 983044
  49.6 8.2 %all-to-all-start = ((bf16[2,80,512]{2,1,0:T(8,128)(2,1)}), bf16[2,80,512]{2,1,0:T(8,128)(2,1)S(1)}, u32[]{:S(2)}, u32[]{:S(2)}) async-start(bf16[2,80,512]{2,1,0:T(8,128)(2,1)} %bitcast.10), calls=%async_computation | async-start | bytes 327680 | tf_op jit(solution)/shard_map/all_to_all | solution.py:122
  53.0 63.3 %all-gather.6.cloned.1.call-start = ((), (), s32[]{:S(2)}) async-start(), calls=%async_computation.3 | async-start | bytes 5570560 | tf_op jit(solution)/shard_map/all_gather | solution.py:133
  57.8 4.2 %copy-start.5 = (f32[80,4]{0,1:T(4,128)S(1)}, f32[80,4]{0,1:T(4,128)}, u32[]{:S(2)}) copy-start(f32[80,4]{0,1:T(4,128)} %param.29) | copy-start | bytes 3844
  57.8 4.2 %copy-start.6 = (s32[80,4]{0,1:T(4,128)S(1)}, s32[80,4]{0,1:T(4,128)}, u32[]{:S(2)}) copy-start(s32[80,4]{0,1:T(4,128)} %param.28) | copy-start | bytes 3844
  61.9 149.7 %reduce-scatter.2.cloned.1.call-start = ((), (), s32[]{:S(2)}) async-start(), calls=%async_computation.4 | async-start | bytes 5570560 | tf_op jit(solution)/shard_map/reduce_scatter | solution.py:139
Sparse Core Ops, SparseCore 0:
  11.9 28.3 all-gather.3
  62.0 54.2 all-gather.5
  134.5 77.0 reduce-scatter.1
where the time goes:
time: 220 us
  waiting for transfers between devices  134 us (61%)
  blocking collectives  29.8 us (14%)
  matrix products  28.3 us (13%)
  between operations  13.4 us (6%)
  other arithmetic  8.51 us (4%)
  starting transfers between devices  3.51 us (2%)
  local copies, waits for them, and re-layouts  2.73 us (1%)
    reduce_scatter x1, waiting for transfers between devices, on_device(): lax.psum_scatter((own_share * product).astype(jnp.bfloat16), ('sp', 'tp')...  77.2 us
    all_gather x1, blocking collectives, on_device(): shares = lax.all_gather(share, ('sp', 'tp'), axis=0, tiled=True)  29.8 us
    all_gather x1, waiting for transfers between devices, on_device(): everyone = lax.all_gather(sent, 'sp', axis=0, tiled=True)  27.4 us
    all_gather x1, waiting for transfers between devices, on_device(): rows = lax.all_gather(normed, ('sp', 'tp'), axis=0, tiled=True)  24.3 us
    dot_general x1, matrix products, on_device(): jnp.dot(active, down_weight[0], preferred_element_type=jnp.float32)  10.5 us
    dot_general x1, matrix products, expert_active(): jnp.dot(rows, gate_w, preferred_element_type=jnp.float32)  7.56 us
    all_to_all x1, waiting for transfers between devices, on_device(): lax.all_to_all(attended.reshape(group, rows_dev, heads_dev * VALUE_WIDTH)...  4.68 us
  transfers between devices with their start and end apart: 4, of which 4 were waited for; matrix products, arithmetic and copies ran while one was open for 1% of the time, Pallas kernels for 0%

commit v1 on v0

--- a/solution.py
+++ b/solution.py
@@ -85,7 +85,6 @@
     latent_width = latent.shape[1]
     sent = jnp.concatenate([normed_latent, key_rot], axis=1)
     everyone = lax.all_gather(sent, "sp", axis=0, tiled=True)
-    shares = lax.all_gather(share, ("sp", "tp"), axis=0, tiled=True)
     all_latent = everyone[:, :latent_width]
     all_rot = everyone[:, latent_width:]
     keys = jnp.dot(all_latent, plain_key_matrix, preferred_element_type=jnp.float32).astype(
@@ -130,7 +129,13 @@
     projected = jnp.dot(own_rows, out_weight, preferred_element_type=jnp.float32)
     hidden = (residual.astype(jnp.float32) + projected).astype(jnp.bfloat16)
     normed = norm_scale(hidden, ffn_gain).astype(jnp.bfloat16)
-    rows = lax.all_gather(normed, ("sp", "tp"), axis=0, tiled=True)
+    shares, rows = jnp.split(
+        lax.all_gather(
+            jnp.concatenate([share, normed], 1), axis_name=("sp", "tp"), axis=0, tiled=True
+        ),
+        [share.shape[1]],
+        axis=1,
+    )
     active = expert_active(rows, gate_weight[0], up_weight[0])
     product = jnp.dot(active, down_weight[0], preferred_element_type=jnp.float32)
     own_share = jnp.sum(

time: 220 us -> 260 us (1.18)
  waiting for transfers between devices: 134 us -> 198 us
  blocking collectives: 29.8 us -> 0 us
    all_gather x1, waiting for transfers between devices: 24.3 us -> 89.7 us  [on_device(): lax.all_gather(jnp.concatenate([share, normed], 1), axis_name=('sp', 'tp'...]
    all_gather x1 -> x0, blocking collectives: 29.8 us -> none  [on_device(): shares = lax.all_gather(share, ('sp', 'tp'), axis=0, tiled=True)]
where the time goes in v1:
time: 260 us; the launch traced here: 259 us
  waiting for transfers between devices  198 us (76%)
  matrix products  30.8 us (12%)
  between operations  13.4 us (5%)
  other arithmetic  10.8 us (4%)
  starting transfers between devices  3.69 us (1%)
  local copies, waits for them, and re-layouts  2.72 us (1%)
    all_gather x1, waiting for transfers between devices, on_device(): lax.all_gather(jnp.concatenate([share, normed], 1), axis_name=('sp', 'tp'...  89.7 us
    reduce_scatter x1, waiting for transfers between devices, on_device(): lax.psum_scatter((own_share * product).astype(jnp.bfloat16), ('sp', 'tp')...  76.8 us
    all_gather x1, waiting for transfers between devices, on_device(): everyone = lax.all_gather(sent, 'sp', axis=0, tiled=True)  26.7 us
    dot_general x1, matrix products, on_device(): jnp.dot(active, down_weight[0], preferred_element_type=jnp.float32)  11.3 us
    dot_general x1, matrix products, expert_active(): jnp.dot(rows, gate_w, preferred_element_type=jnp.float32)  9.21 us
  transfers between devices with their start and end apart: 4, of which 4 were waited for; matrix products, arithmetic and copies ran while one was open for 1% of the time, Pallas kernels for 0%

profile of v1, /device:TPU:0, one launch (start us, length us, event | category | flops | bytes accessed | tf_op | source)
XLA Modules:
  0.0 259.2 jit_solution(1321712183640586577)
XLA Ops:
  6.6 1.2 fusion.58
  7.8 0.7 convert_element_type.95
  8.5 0.8 convert_element_type.97
  9.2 0.2 multiply_cosine_fusion
  9.5 0.1 copy.43
  9.6 0.1 copy.42
  9.7 0.1 copy.44
  9.8 0.1 copy.45
  9.9 1.0 fusion.60
  11.0 0.8 concatenate.16
  11.8 0.0 all-gather.3.cloned.1.call-update
  11.8 0.7 convert_element_type.112
  12.5 1.0 copy.46
  13.6 26.7 %all-gather.3.cloned.1.call-done = bf16[1280,576]{1,0:T(8,128)(2,1)} async-done(((bf16[160,576]{1,0:T(8,128)(2,1)}), bf16[1280,576]{1,0:T(8,128)(2,1)}) %all-gather.3.cloned.1.call-update) | async-done | bytes 1474576 | tf_op jit(solution)/shard_map/all_gather | solution.py:87
  40.3 2.2 convolution_convert_fusion.1
  42.5 0.3 convolution_bitcast_fusion
  42.8 0.3 convolution_bitcast_fusion.1
  43.0 0.3 convolution_bitcast_fusion.2
  43.3 0.3 convolution_bitcast_fusion.3
  43.6 0.3 copy-done.1
  43.9 0.4 fusion.85
  44.3 0.3 fusion.47
  44.6 0.8 convolution_convert_fusion
  45.5 0.3 fusion.36
  45.8 0.4 fusion.86
  46.2 0.3 fusion.45
  46.5 0.3 fusion.35
  46.8 0.4 fusion.88
  47.2 0.3 fusion.41
  47.5 0.3 fusion.33
  47.9 0.4 fusion.87
  48.3 0.3 fusion.43
  48.6 0.3 fusion.34
  48.9 0.7 pad_maximum_fusion.1
  49.6 3.4 %all-to-all-start = ((bf16[2,80,512]{2,1,0:T(8,128)(2,1)}), bf16[2,80,512]{2,1,0:T(8,128)(2,1)S(1)}, u32[]{:S(2)}, u32[]{:S(2)}) async-start(bf16[2,80,512]{2,1,0:T(8,128)(2,1)} %bitcast.10), calls=%async_computation | async-start | bytes 327680 | tf_op jit(solution)/shard_map/all_to_all | solution.py:121
  53.0 0.0 all-gather.5.cloned.1.call-start
  53.1 0.1 copy.48
  53.2 4.6 %all-to-all-done = bf16[2,80,512]{2,1,0:T(8,128)(2,1)S(1)} async-done(((bf16[2,80,512]{2,1,0:T(8,128)(2,1)}), bf16[2,80,512]{2,1,0:T(8,128)(2,1)S(1)}, u32[]{:S(2)}, u32[]{:S(2)}) %all-to-all-start) | async-done | bytes 163872 | tf_op jit(solution)/shard_map/all_to_all | solution.py:121
  57.8 3.2 %multiply_reduce_fusion = (f32[80]{0:T(128)S(1)}, f32[80,2048]{1,0:T(8,128)S(1)}) fusion(bf16[80,1024]{1,0:T(8,128)(2,1)S(1)} %bitcast.49, bf16[1024,2048]{1,0:T(8,128)(2,1)} %param.23, bf16[80,2048]{1,0:T(8,128)(2,1)S(1)} %copy-done.2), kind=kOutput, calls=%fused_computation.58 | convolution fusion | flops 336527296 | bytes 5341504 | tf_op jit(solution)/shard_map/dot_general | solution.py:129
  61.0 0.1 fusion.61
  61.1 1.1 pad_maximum_fusion
  62.3 0.2 reduce-scatter.2.cloned.1.call-start
  62.5 89.7 %all-gather.5.cloned.1.call-done = f32[1280,2056]{1,0:T(8,128)} async-done(((f32[80,2056]{1,0:T(8,128)}), f32[1280,2056]{1,0:T(8,128)}) %all-gather.5.cloned.1.call-update) | async-done | bytes 10526736 | tf_op jit(solution)/shard_map/all_gather | solution.py:133
  152.2 1.3 fusion.49
  153.6 9.2 %fusion.7 = f32[1280,512]{1,0:T(8,128)} fusion(f32[1280,2056]{1,0:T(8,128)} %all-gather.5.cloned.1.call-done, bf16[1,2048,512]{2,1,0:T(8,128)(2,1)} %param.25), kind=kOutput, calls=%fused_computation.6 | convolution fusion | flops 2685009920 | bytes 9961472 | tf_op jit(solution)/shard_map/dot_general | solution.py:51
  162.8 11.3 %multiply_convert_fusion = bf16[1280,2048]{1,0:T(8,128)(2,1)} fusion(f32[1280]{0:T(1024)S(1)} %fusion.49, bf16[1,512,2048]{2,1,0:T(8,128)(2,1)S(1)} %copy-done, f32[1280,512]{1,0:T(8,128)} %fusion.7, f32[1280,2056]{1,0:T(8,128)} %all-gather.5.cloned.1.call-done, bf16[1,2048,512]{2,1,0:T(8,128)(2,1)} %param.26), kind=kOutput, calls=%fused_computation | convolution fusion | flops 5379850240 | bytes 17306624 | tf_op jit(solution)/shard_map/dot_general | solution.py:140
  174.1 76.8 %reduce-scatter.2.cloned.1.call-done = bf16[80,2048]{1,0:T(8,128)(2,1)} async-done(((bf16[1280,2048]{1,0:T(8,128)(2,1)}), bf16[80,2048]{1,0:T(8,128)(2,1)}) %reduce-scatter.2.cloned.1.call-update) | async-done | bytes 327696 | tf_op jit(solution)/shard_map/reduce_scatter | solution.py:144
  250.9 1.8 add_convert_fusion
  (28 shorter events, 0.2 us)
Async XLA Ops:
  6.5 156.2 %copy-start = (bf16[1,512,2048]{2,1,0:T(8,128)(2,1)S(1)}, bf16[1,512,2048]{2,1,0:T(8,128)(2,1)}, u32[]{:S(2)}) copy-start(bf16[1,512,2048]{2,1,0:T(8,128)(2,1)} %param.27) | copy-start | bytes 6291460
  6.5 33.8 %copy-start.6 = (bf16[512,512]{1,0:T(8,128)(2,1)S(1)}, bf16[512,512]{1,0:T(8,128)(2,1)}, u32[]{:S(2)}) copy-start(bf16[512,512]{1,0:T(8,128)(2,1)} %param.20) | copy-start | bytes 1572868
  6.5 33.8 %all-gather.3.cloned.1.call-start = ((), (), s32[]{:S(2)}) async-start(), calls=%async_computation.2 | async-start | bytes 1843200 | tf_op jit(solution)/shard_map/all_gather | solution.py:87
  13.6 28.9 %copy-start.3 = (bf16[160,512]{1,0:T(8,128)(2,1)S(1)}, bf16[160,512]{1,0:T(8,128)(2,1)}, u32[]{:S(2)}) copy-start(bf16[160,512]{1,0:T(8,128)(2,1)} %param.15) | copy-start | bytes 491524
  42.5 1.4 copy-start.1
  43.3 1.3 copy-start.7
  47.8 5.2 %copy-start.4 = (f32[80,4]{0,1:T(4,128)S(1)}, f32[80,4]{0,1:T(4,128)}, u32[]{:S(2)}) copy-start(f32[80,4]{0,1:T(4,128)} %param.29) | copy-start | bytes 3844
  47.9 5.2 %copy-start.5 = (s32[80,4]{0,1:T(4,128)S(1)}, s32[80,4]{0,1:T(4,128)}, u32[]{:S(2)}) copy-start(s32[80,4]{0,1:T(4,128)} %param.28) | copy-start | bytes 3844
  47.9 9.9 %copy-start.2 = (bf16[80,2048]{1,0:T(8,128)(2,1)S(1)}, bf16[80,2048]{1,0:T(8,128)(2,1)}, u32[]{:S(2)}) copy-start(bf16[80,2048]{1,0:T(8,128)(2,1)} %param.22) | copy-start | bytes 983044
  49.6 8.2 %all-to-all-start = ((bf16[2,80,512]{2,1,0:T(8,128)(2,1)}), bf16[2,80,512]{2,1,0:T(8,128)(2,1)S(1)}, u32[]{:S(2)}, u32[]{:S(2)}) async-start(bf16[2,80,512]{2,1,0:T(8,128)(2,1)} %bitcast.10), calls=%async_computation | async-start | bytes 327680 | tf_op jit(solution)/shard_map/all_to_all | solution.py:121
  53.0 99.2 %all-gather.5.cloned.1.call-start = ((), (), s32[]{:S(2)}) async-start(), calls=%async_computation.3 | async-start | bytes 11837440 | tf_op jit(solution)/shard_map/all_gather | solution.py:133
  62.3 188.6 %reduce-scatter.2.cloned.1.call-start = ((), (), s32[]{:S(2)}) async-start(), calls=%async_computation.4 | async-start | bytes 5570560 | tf_op jit(solution)/shard_map/reduce_scatter | solution.py:144
Sparse Core Ops, SparseCore 0:
  11.9 28.3 all-gather.2
  62.4 89.8 all-gather.4
  174.3 76.6 reduce-scatter.1
